TPU v7x, 512 devices: a whole 4x8x8 slice. The times are simulated.
512 devices in a mesh: sp: 64 (over z, y), tp: 4 (over x), dp: 2 (over core).
Axes of the slice: x: 4, y: 8, z: 8, core: 2. Of those that a mesh axis runs over, the one named last changes fastest.
Arguments:
- latent: bfloat16 [2, 16384, 2048], P('dp', 'sp'), may hold values from -1.5 to 1.5
- condition: bfloat16 [2, 2048], P('dp', 'sp'), may hold values from -6 to 6
- context: bfloat16 [2, 1024, 2048], P('dp', 'sp'), may hold values from -6 to 6
- context_code: bfloat16 [2048], P('sp'), may hold values from -6 to 6
- shift_weight: bfloat16 [2048, 2048], P('sp', 'tp'), may hold values from -0.125 to 0.125
- scale_weight: bfloat16 [2048, 2048], P('sp', 'tp'), may hold values from -0.125 to 0.125
- gate_weight: bfloat16 [2048, 2048], P('sp', 'tp'), may hold values from -0.125 to 0.125
- norm_gain: float32 [2048], replicated, may hold values from 0.1 to 1.9
- query_weight: bfloat16 [2048, 1024], P(None, 'tp'), may hold values from -0.125 to 0.125
- key_weight: bfloat16 [2048, 256], P(None, 'tp'), may hold values from -0.125 to 0.125
- value_weight: bfloat16 [2048, 256], P(None, 'tp'), may hold values from -0.125 to 0.125
- output_weight: bfloat16 [1024, 2048], P('tp'), may hold values from -0.75 to 0.75
- query_gain: float32 [64], replicated, may hold values from 1 to 5.5
- key_gain: float32 [64], replicated, may hold values from 1 to 5.5
- context_bias: float32 [16], P('tp'), may hold values from 0.5 to 2
Outputs:
- updated: bfloat16 [2, 16384, 2048], P('dp', 'sp')
All inputs are finite; a program needn't handle non-finite values.
Results may differ from a plain program's by a relative error of at most 0.01405.
The roundings to bfloat16 on the way count: a program that leaves them out, or rounds other values in their place, can miss the bound.
Values may be sent and summed in bfloat16 or wider, within the bound.
A program may use at most 64 MiB of HBM per device.

v0:
```python
import math
import jax
import jax.numpy as jnp
from jax import lax
from jax.sharding import PartitionSpec as P

GRID_W = 64
norm_eps = 1e-06
rope_base = 10000.0


def from_everyone(array, axis):
    size = lax.axis_size(axis)
    return lax.all_to_all(
        jnp.broadcast_to(array[None], (size, *array.shape)), axis, 0, 0, tiled=True
    )


def of_everyone(array, axis):
    return from_everyone(array, axis).sum(axis=0)


def laid_out(pieces, dim):
    dims = list(pieces.shape[1:])
    dims[dim] *= pieces.shape[0]
    return jnp.moveaxis(pieces, 0, dim).reshape(dims)


def gathered_copies(array, axis, dim):
    pieces = from_everyone(array, axis)
    return laid_out(pieces, dim)


def cut_along(array, dim, size):
    before, after = (array.shape[:dim], array.shape[dim + 1 :])
    return jnp.moveaxis(array.reshape(*before, size, -1, *after), dim, 0)


def sent_and_summed(array, axis, dim):
    size = lax.axis_size(axis)
    pieces = lax.all_to_all(cut_along(array, dim, size), axis, 0, 0, tiled=True)
    return jnp.sum(pieces.astype(jnp.float32), axis=0)


def rotary_tables(position, grid_width, head_dim):
    grid_row = (position // grid_width).astype(jnp.float32)
    grid_col = (position % grid_width).astype(jnp.float32)
    quarter = head_dim // 4
    inverse = rope_base ** (-jnp.arange(quarter, dtype=jnp.float32) / quarter)
    angles = jnp.concatenate([grid_row[:, None] * inverse, grid_col[:, None] * inverse], axis=-1)
    return (jnp.cos(angles), jnp.sin(angles))


def head_norm(values, gain_row):
    return (
        values * lax.rsqrt(jnp.mean(values * values, axis=-1, keepdims=True) + norm_eps) * gain_row
    )


def rotate(values, cosine, sine_part):
    half_dim = values.shape[-1] // 2
    first_half = values[..., :half_dim]
    second_half = values[..., half_dim:]
    cos_rows = cosine[:, None, :]
    sin_rows = sine_part[:, None, :]
    return jnp.concatenate(
        [
            first_half * cos_rows - second_half * sin_rows,
            second_half * cos_rows + first_half * sin_rows,
        ],
        axis=-1,
    )


def modulated(tokens, gain_row, shift_row, scale_row):
    floats = tokens.astype(jnp.float32)
    normal = floats * lax.rsqrt(jnp.mean(floats * floats, axis=-1, keepdims=True) + norm_eps)
    return (normal * gain_row * (1.0 + scale_row) + shift_row).astype(jnp.bfloat16)


def on_device(
    latent,
    condition,
    context,
    context_code,
    shift_weight,
    scale_weight,
    gate_weight,
    norm_gain,
    query_weight,
    key_weight,
    value_weight,
    output_weight,
    query_gain,
    key_gain,
    context_bias,
):
    head_dim = query_gain.shape[0]
    tp_size = lax.axis_size("tp")
    activated = jax.nn.silu(condition[0].astype(jnp.float32)).astype(jnp.bfloat16)
    context_act = jax.nn.silu(context_code.astype(jnp.float32)).astype(jnp.bfloat16)
    partial_mod = jnp.stack(
        [
            jnp.dot(activated, shift_weight, preferred_element_type=jnp.float32),
            jnp.dot(activated, scale_weight, preferred_element_type=jnp.float32),
            jnp.dot(activated, gate_weight, preferred_element_type=jnp.float32),
            jnp.dot(context_act, shift_weight, preferred_element_type=jnp.float32),
            jnp.dot(context_act, scale_weight, preferred_element_type=jnp.float32),
        ]
    )
    summed = of_everyone(partial_mod, "sp")
    vectors = gathered_copies(summed, "tp", 1)
    normed = modulated(latent[0], norm_gain, vectors[0], vectors[1])
    query_cols = query_weight.shape[1]
    key_cols = key_weight.shape[1]
    projected = jnp.concatenate(
        [
            jnp.dot(normed, query_weight, preferred_element_type=jnp.float32),
            jnp.dot(normed, key_weight, preferred_element_type=jnp.float32),
            jnp.dot(normed, value_weight, preferred_element_type=jnp.float32),
        ],
        axis=1,
    )
    seq_rows = projected.shape[0]
    position = lax.axis_index("sp") * seq_rows + jnp.arange(seq_rows, dtype=jnp.int32)
    cosine, sine_part = rotary_tables(position, GRID_W, head_dim)
    group_size = query_cols // head_dim
    queries = projected[:, :query_cols].reshape(seq_rows, group_size, head_dim)
    queries = rotate(head_norm(queries, query_gain), cosine, sine_part).astype(jnp.bfloat16)
    latent_keys = projected[:, query_cols : query_cols + key_cols].reshape(seq_rows, 1, head_dim)
    latent_keys = rotate(head_norm(latent_keys, key_gain), cosine, sine_part).astype(jnp.bfloat16)
    latent_values = projected[:, query_cols + key_cols :].astype(jnp.bfloat16)
    key_value = jnp.concatenate([latent_keys.reshape(seq_rows, head_dim), latent_values], axis=1)
    context_normed = modulated(context[0], norm_gain, vectors[3], vectors[4])
    context_keys = head_norm(
        jnp.dot(context_normed, key_weight, preferred_element_type=jnp.float32), key_gain
    )
    context_values = jnp.dot(context_normed, value_weight, preferred_element_type=jnp.float32)
    context_kv = gathered_copies(
        jnp.concatenate(
            [context_keys.astype(jnp.bfloat16), context_values.astype(jnp.bfloat16)], axis=1
        ),
        "sp",
        0,
    )
    score_scale = head_dim ** (-0.5)
    query_rows = queries.transpose(1, 0, 2).reshape(group_size * seq_rows, head_dim)
    bias_rows = jnp.repeat(context_bias, seq_rows)
    context_scores = jnp.dot(
        query_rows, context_kv[:, :head_dim].T, preferred_element_type=jnp.float32
    )
    context_scores = context_scores * score_scale + bias_rows[:, None]
    first_max = context_scores.max(axis=1)
    context_exp = jnp.exp(context_scores - first_max[:, None])
    start_state = (
        first_max,
        context_exp.sum(axis=1),
        jnp.dot(
            context_exp.astype(jnp.bfloat16),
            context_kv[:, head_dim:],
            preferred_element_type=jnp.float32,
        ),
    )
    arrived = lax.all_gather(key_value, "sp", axis=0, tiled=True)
    arrived_rows = arrived.shape[0]
    block_rows = math.gcd(arrived_rows, 1024)
    blocks = arrived.reshape(arrived_rows // block_rows, block_rows, 2 * head_dim)

    def absorb_block(state_now, pair_block):
        old_max, old_total, old_accum = state_now
        scores = (
            jnp.dot(query_rows, pair_block[:, :head_dim].T, preferred_element_type=jnp.float32)
            * score_scale
        )
        new_max = jnp.maximum(old_max, scores.max(axis=1))
        factor = jnp.exp(old_max - new_max)
        weights = jnp.exp(scores - new_max[:, None])
        new_accum = old_accum * factor[:, None] + jnp.dot(
            weights.astype(jnp.bfloat16),
            pair_block[:, head_dim:],
            preferred_element_type=jnp.float32,
        )
        return ((new_max, old_total * factor + weights.sum(axis=1), new_accum), None)

    final_state, unused = lax.scan(absorb_block, start_state, blocks)
    row_max, totals, accum = final_state
    attended = (accum / totals[:, None]).astype(jnp.bfloat16)
    attended = (
        attended.reshape(group_size, seq_rows, head_dim)
        .transpose(1, 0, 2)
        .reshape(seq_rows, query_cols)
    )
    own_rows = seq_rows // tp_size
    mixed = sent_and_summed(
        jnp.dot(attended, output_weight, preferred_element_type=jnp.float32).astype(jnp.bfloat16),
        "tp",
        0,
    )
    own_latent = lax.dynamic_slice_in_dim(latent[0], lax.axis_index("tp") * own_rows, own_rows, 0)
    updated = (own_latent.astype(jnp.float32) + vectors[2] * mixed).astype(jnp.bfloat16)
    whole = gathered_copies(updated, "tp", 0)
    return whole[None]


def solution(mesh):
    return jax.shard_map(
        on_device,
        mesh=mesh,
        in_specs=(
            P("dp", "sp", None),
            P("dp", "sp"),
            P("dp", "sp", None),
            P("sp"),
            P("sp", "tp"),
            P("sp", "tp"),
            P("sp", "tp"),
            P(),
            P(None, "tp"),
            P(None, "tp"),
            P(None, "tp"),
            P("tp", None),
            P(),
            P(),
            P("tp"),
        ),
        out_specs=P("dp", "sp", None),
        check_vma=False,
    )
```

profile of v0, /device:TPU:8, one launch (start us, length us, event | category | flops | bytes accessed | tf_op | source)
XLA Modules:
  0.0 259.9 jit_solution(298645395595733858)
XLA Ops:
  6.5 1.0 fusion.59
  11.3 1.1 broadcast_in_dim.12
  12.4 16.6 %all-to-all-start = ((f32[64,5,512]{2,1,0:T(8,128)}), f32[64,5,512]{2,1,0:T(8,128)S(1)}, u32[]{:S(2)}, u32[]{:S(2)}) async-start(f32[64,5,512]{2,1,0:T(8,128)} %broadcast_in_dim.12), calls=%async_computation | async-start | bytes 2097152 | tf_op jit(solution)/shard_map/all_to_all | solution.py:14
  29.0 2.1 fusion.16
  31.2 27.1 %all-to-all-done = f32[64,5,512]{2,1,0:T(8,128)S(1)} async-done(((f32[64,5,512]{2,1,0:T(8,128)}), f32[64,5,512]{2,1,0:T(8,128)S(1)}, u32[]{:S(2)}, u32[]{:S(2)}) %all-to-all-start) | async-done | bytes 655392 | tf_op jit(solution)/shard_map/all_to_all | solution.py:14
  59.0 4.3 %all-to-all-start.1 = ((f32[4,5,512]{2,1,0:T(8,128)}), f32[4,5,512]{2,1,0:T(8,128)S(1)}, u32[]{:S(2)}, u32[]{:S(2)}) async-start(f32[4,5,512]{2,1,0:T(8,128)} %broadcast_in_dim.13), calls=%async_computation.1 | async-start | bytes 131072 | tf_op jit(solution)/shard_map/all_to_all | solution.py:14
  63.3 1.3 add_rsqrt_fusion.2
  64.6 4.3 %all-to-all-done.1 = f32[4,5,512]{2,1,0:T(8,128)S(1)} async-done(((f32[4,5,512]{2,1,0:T(8,128)}), f32[4,5,512]{2,1,0:T(8,128)S(1)}, u32[]{:S(2)}, u32[]{:S(2)}) %all-to-all-start.1) | async-done | bytes 40992 | tf_op jit(solution)/shard_map/all_to_all | solution.py:14
  69.5 1.6 convolution_convert_fusion.1
  71.2 1.3 multiply_reduce_fusion.2
  74.8 1.4 copy.33
  76.5 1.1 multiply_reduce_fusion.3
  78.3 1.2 convolution_convert_fusion.2
  80.3 7.0 %all-to-all-start.2 = ((bf16[64,16,128]{2,1,0:T(8,128)(2,1)}), bf16[64,16,128]{2,1,0:T(8,128)(2,1)S(1)}, u32[]{:S(2)}, u32[]{:S(2)}) async-start(bf16[64,16,128]{2,1,0:T(8,128)(2,1)} %broadcast_in_dim.14), calls=%async_computation.2 | async-start | bytes 524288 | tf_op jit(solution)/shard_map/all_to_all | solution.py:14
  87.3 2.0 multiply_reduce_fusion.1
  89.7 10.9 %all-to-all-done.2 = bf16[64,16,128]{2,1,0:T(8,128)(2,1)S(1)} async-done(((bf16[64,16,128]{2,1,0:T(8,128)(2,1)}), bf16[64,16,128]{2,1,0:T(8,128)(2,1)S(1)}, u32[]{:S(2)}, u32[]{:S(2)}) %all-to-all-start.2) | async-done | bytes 262176 | tf_op jit(solution)/shard_map/all_to_all | solution.py:14
  102.1 1.0 fusion.25
  103.1 57.5 %all-gather.2.cloned.1.call-done = bf16[16384,128]{0,1:T(8,128)(2,1)} async-done(((bf16[256,128]{0,1:T(8,128)(2,1)}), bf16[16384,128]{0,1:T(8,128)(2,1)}) %all-gather.2.cloned.1.call-update) | async-done | bytes 4194320 | tf_op jit(solution)/shard_map/all_gather | solution.py:164
  160.6 6.4 %copy.38 = bf16[16384,128]{1,0:T(8,128)(2,1)} copy(bf16[16384,128]{0,1:T(8,128)(2,1)} %all-gather.2.cloned.1.call-done) | data formatting | bytes 8388608 | tf_op jit(solution)/shard_map/while | solution.py:185
  167.0 54.7 %while.14 = (s32[]{:T(128)}, f32[1024]{0:T(1024)S(1)}, f32[1024]{0:T(1024)S(1)}, f32[1024,64]{0,1:T(8,128)S(1)}, bf16[16,1024,128]{2,1,0:T(8,128)(2,1)}, /*index=5*/bf16[1024,64]{1,0:T(8,128)(2,1)S(1)}, s32[]{:T(128)}) while((s32[]{:T(128)}, f32[1024]{0:T(1024)S(1)}, f32[1024]{0:T(1024)S(1)}, f32[1024,64]{0,1:T(8,128)S(1)}, ...), condition=%wide.region_11.12_spmd, body=%wide.region_8.11_spmd.sunk | while | flops 276957184 | bytes 14352473 | solution.py:185
  167.0 1.0 dynamic-slice_bitcast_fusion.2
  170.4 1.0 dynamic-slice_bitcast_fusion.2
  173.8 1.0 dynamic-slice_bitcast_fusion.2
  176.3 0.9 fusion.105
  177.2 1.0 dynamic-slice_bitcast_fusion.2
  179.7 0.9 fusion.105
  180.7 1.0 dynamic-slice_bitcast_fusion.2
  183.1 0.9 fusion.105
  184.1 1.0 dynamic-slice_bitcast_fusion.2
  186.5 0.9 fusion.105
  187.5 1.0 dynamic-slice_bitcast_fusion.2
  190.0 0.9 fusion.105
  190.9 1.0 dynamic-slice_bitcast_fusion.2
  193.4 0.9 fusion.105
  194.3 1.0 dynamic-slice_bitcast_fusion.2
  196.8 0.9 fusion.105
  197.8 1.0 dynamic-slice_bitcast_fusion.2
  201.2 1.0 dynamic-slice_bitcast_fusion.2
  204.6 1.0 dynamic-slice_bitcast_fusion.2
  208.0 1.0 dynamic-slice_bitcast_fusion.2
  211.4 1.0 dynamic-slice_bitcast_fusion.2
  214.9 1.0 dynamic-slice_bitcast_fusion.2
  218.3 1.0 dynamic-slice_bitcast_fusion.2
  221.9 1.4 convolution_convert_fusion
  223.3 4.2 %all-to-all-start.3 = ((bf16[4,64,2048]{2,1,0:T(8,128)(2,1)}), bf16[4,64,2048]{2,1,0:T(8,128)(2,1)S(1)}, u32[]{:S(2)}, u32[]{:S(2)}) async-start(bf16[4,64,2048]{2,1,0:T(8,128)(2,1)} %bitcast.36), calls=%async_computation.3 | async-start | bytes 2097152 | tf_op jit(solution)/shard_map/all_to_all | solution.py:41
  227.5 10.9 %all-to-all-done.3 = bf16[4,64,2048]{2,1,0:T(8,128)(2,1)S(1)} async-done(((bf16[4,64,2048]{2,1,0:T(8,128)(2,1)}), bf16[4,64,2048]{2,1,0:T(8,128)(2,1)S(1)}, u32[]{:S(2)}, u32[]{:S(2)}) %all-to-all-start.3) | async-done | bytes 1048608 | tf_op jit(solution)/shard_map/all_to_all | solution.py:41
  238.8 13.3 %all_to_all.25 = bf16[4,64,2048]{2,1,0:T(8,128)(2,1)S(1)} all-to-all(bf16[4,64,2048]{2,1,0:T(8,128)(2,1)S(1)} %broadcast_in_dim.17), channel_id=1, replica_groups=mesh['sp'=64,'tp'=4,'dp'=2] {'tp'}, dimensions={0} | all-to-all | bytes 2097152 | tf_op jit(solution)/shard_map/all_to_all | solution.py:14
  252.1 1.0 copy.55
  (147 shorter events, 43.4 us)
Async XLA Ops:
  6.5 215.3 %copy-start = (bf16[256,2048]{1,0:T(8,128)(2,1)S(1)}, bf16[256,2048]{1,0:T(8,128)(2,1)}, u32[]{:S(2)}) copy-start(bf16[256,2048]{1,0:T(8,128)(2,1)} %param.28) | copy-start | bytes 3145732
  6.5 63.0 %copy-start.1 = (bf16[1,256,2048]{2,1,0:T(8,128)(2,1)S(1)}, bf16[1,256,2048]{2,1,0:T(8,128)(2,1)}, u32[]{:S(2)}) copy-start(bf16[1,256,2048]{2,1,0:T(8,128)(2,1)} %param.17) | copy-start | bytes 3145732
  11.2 59.9 %copy-start.4 = (bf16[2048,64]{0,1:T(8,128)(2,1)S(1)}, bf16[2048,64]{0,1:T(8,128)(2,1)}, u32[]{:S(2)}) copy-start(bf16[2048,64]{0,1:T(8,128)(2,1)} %param.26) | copy-start | bytes 786436
  12.4 45.9 %all-to-all-start = ((f32[64,5,512]{2,1,0:T(8,128)}), f32[64,5,512]{2,1,0:T(8,128)S(1)}, u32[]{:S(2)}, u32[]{:S(2)}) async-start(f32[64,5,512]{2,1,0:T(8,128)} %broadcast_in_dim.12), calls=%async_computation | async-start | bytes 2097152 | tf_op jit(solution)/shard_map/all_to_all | solution.py:14
  58.3 16.5 %copy-start.2 = (bf16[2048,256]{1,0:T(8,128)(2,1)S(1)}, bf16[2048,256]{1,0:T(8,128)(2,1)}, u32[]{:S(2)}) copy-start(bf16[2048,256]{1,0:T(8,128)(2,1)} %param.25) | copy-start | bytes 3145732
  59.0 9.9 %all-to-all-start.1 = ((f32[4,5,512]{2,1,0:T(8,128)}), f32[4,5,512]{2,1,0:T(8,128)S(1)}, u32[]{:S(2)}, u32[]{:S(2)}) async-start(f32[4,5,512]{2,1,0:T(8,128)} %broadcast_in_dim.13), calls=%async_computation.1 | async-start | bytes 131072 | tf_op jit(solution)/shard_map/all_to_all | solution.py:14
  63.3 97.3 %all-gather.2.cloned.1.call-start = ((), (), s32[]{:S(2)}) async-start(), calls=%async_computation.5 | async-start | bytes 4259840 | tf_op jit(solution)/shard_map/all_gather | solution.py:164
  69.5 3.9 %copy-start.6 = (f32[1,4,512]{2,0,1:T(1,128)}, f32[1,4,512]{2,0,1:T(1,128)S(1)}, u32[]{:S(2)}) copy-start(f32[1,4,512]{2,0,1:T(1,128)S(1)} %get-tuple-element.93) | copy-start | bytes 24580
  69.5 3.9 %copy-start.7 = (f32[1,4,512]{2,0,1:T(1,128)}, f32[1,4,512]{2,0,1:T(1,128)S(1)}, u32[]{:S(2)}) copy-start(f32[1,4,512]{2,0,1:T(1,128)S(1)} %get-tuple-element.94) | copy-start | bytes 24580
  69.5 6.8 %copy-start.3 = (bf16[1,16,2048]{2,1,0:T(8,128)(2,1)S(1)}, bf16[1,16,2048]{2,1,0:T(8,128)(2,1)}, u32[]{:S(2)}) copy-start(bf16[1,16,2048]{2,1,0:T(8,128)(2,1)} %param.19) | copy-start | bytes 196612
  74.8 14.5 %copy-start.8 = (f32[64]{0:T(128)S(1)}, f32[64]{0:T(128)}, u32[]{:S(2)}) copy-start(f32[64]{0:T(128)} %param.29) | copy-start | bytes 772
  80.3 20.2 %all-to-all-start.2 = ((bf16[64,16,128]{2,1,0:T(8,128)(2,1)}), bf16[64,16,128]{2,1,0:T(8,128)(2,1)S(1)}, u32[]{:S(2)}, u32[]{:S(2)}) async-start(bf16[64,16,128]{2,1,0:T(8,128)(2,1)} %broadcast_in_dim.14), calls=%async_computation.2 | async-start | bytes 524288 | tf_op jit(solution)/shard_map/all_to_all | solution.py:14
  221.7 16.9 %copy-start.5 = (f32[1,4,512]{2,0,1:T(1,128)S(1)}, f32[1,4,512]{2,0,1:T(1,128)}, u32[]{:S(2)}) copy-start(f32[1,4,512]{2,0,1:T(1,128)} %get-tuple-element.90) | copy-start | bytes 24580
  223.3 15.1 %all-to-all-start.3 = ((bf16[4,64,2048]{2,1,0:T(8,128)(2,1)}), bf16[4,64,2048]{2,1,0:T(8,128)(2,1)S(1)}, u32[]{:S(2)}, u32[]{:S(2)}) async-start(bf16[4,64,2048]{2,1,0:T(8,128)(2,1)} %bitcast.36), calls=%async_computation.3 | async-start | bytes 2097152 | tf_op jit(solution)/shard_map/all_to_all | solution.py:41
Sparse Core Ops, SparseCore 0:
  74.2 86.3 all-gather.1
where the time goes:
time: 261 us; the launch traced here: 260 us
  waiting for transfers between devices  111 us (43%)
  matrix products  41.4 us (16%)
  starting transfers between devices  32.1 us (12%)
  local copies, waits for them, and re-layouts  28 us (11%)
  other arithmetic  20 us (8%)
  between operations  13.7 us (5%)
  blocking collectives  13.3 us (5%)
    all_gather x1, waiting for transfers between devices, on_device(): arrived = lax.all_gather(key_value, 'sp', axis=0, tiled=True)  57.5 us
    all_to_all x3, waiting for transfers between devices, from_everyone(): lax.all_to_all(jnp.broadcast_to(array[None], (size, *array.shape)), axis,...  42.3 us
    all_to_all x3, starting transfers between devices, from_everyone(): lax.all_to_all(jnp.broadcast_to(array[None], (size, *array.shape)), axis,...  27.8 us
    squeeze x16, local copies, waits for them, and re-layouts, on_device(): final_state, unused = lax.scan(absorb_block, start_state, blocks)  15.5 us
    dot_general x16, matrix products, absorb_block(): jnp.dot(weights.astype(jnp.bfloat16), pair_block[:, head_dim:], preferred...  14.9 us
    all_to_all x1, blocking collectives, from_everyone(): lax.all_to_all(jnp.broadcast_to(array[None], (size, *array.shape)), axis,...  13.3 us
    reduce_sum x16, other arithmetic, absorb_block(): weights.sum(axis=1)  11.7 us
    dot_general x16, matrix products, absorb_block(): jnp.dot(query_rows, pair_block[:, :head_dim].T, preferred_element_type=jn...  11.5 us
  transfers between devices with their start and end apart: 5, of which 5 were waited for; matrix products, arithmetic and copies ran while one was open for 6% of the time, Pallas kernels for 0%

commit v1 on v0

--- a/solution.py
+++ b/solution.py
@@ -7,6 +7,18 @@
 GRID_W = 64
 norm_eps = 1e-06
 rope_base = 10000.0
+
+
+def gather_by_bits(x, axis, dim):
+    ways, here = (lax.axis_size(axis), lax.axis_index(axis))
+    grown, reach = (x, 1)
+    while reach < ways:
+        theirs = lax.ppermute(grown, axis, [(d, d ^ reach) for d in range(ways)])
+        mine_first = jnp.concatenate([grown, theirs], axis=dim)
+        theirs_first = jnp.concatenate([theirs, grown], axis=dim)
+        grown = jnp.where(here & reach == 0, mine_first, theirs_first)
+        reach = 2 * reach
+    return grown
 
 
 def from_everyone(array, axis):
@@ -161,7 +173,7 @@
             preferred_element_type=jnp.float32,
         ),
     )
-    arrived = lax.all_gather(key_value, "sp", axis=0, tiled=True)
+    arrived = gather_by_bits(key_value, "sp", 0)
     arrived_rows = arrived.shape[0]
     block_rows = math.gcd(arrived_rows, 1024)
     blocks = arrived.reshape(arrived_rows // block_rows, block_rows, 2 * head_dim)

time: 261 us -> 362 us (1.39)
  the two profiles are of different devices: /device:TPU:8 before, /device:TPU:192 now
where the time goes in v1:
time: 362 us; the launch traced here: 360 us
  waiting for transfers between devices  189 us (52%)
  starting transfers between devices  53.5 us (15%)
  matrix products  40.1 us (11%)
  local copies, waits for them, and re-layouts  30.1 us (8%)
  other arithmetic  29.2 us (8%)
  blocking collectives  16.8 us (5%)
    ppermute x6, waiting for transfers between devices, gather_by_bits(): theirs = lax.ppermute(grown, axis, [(d, d ^ reach) for d in range(ways)])  141 us
    all_to_all x3, waiting for transfers between devices, from_everyone(): lax.all_to_all(jnp.broadcast_to(array[None], (size, *array.shape)), axis,...  32.6 us
    all_to_all x3, starting transfers between devices, from_everyone(): lax.all_to_all(jnp.broadcast_to(array[None], (size, *array.shape)), axis,...  29.5 us
    ppermute x6, starting transfers between devices, gather_by_bits(): theirs = lax.ppermute(grown, axis, [(d, d ^ reach) for d in range(ways)])  20.5 us
    all_to_all x1, blocking collectives, from_everyone(): lax.all_to_all(jnp.broadcast_to(array[None], (size, *array.shape)), axis,...  16.8 us
    squeeze x16, local copies, waits for them, and re-layouts, on_device(): final_state, unused = lax.scan(absorb_block, start_state, blocks)  15.5 us
    all_to_all x1, waiting for transfers between devices, sent_and_summed(): pieces = lax.all_to_all(cut_along(array, dim, size), axis, 0, 0, tiled=True)  15.2 us
    dot_general x16, matrix products, absorb_block(): jnp.dot(weights.astype(jnp.bfloat16), pair_block[:, head_dim:], preferred...  14.9 us
  transfers between devices with their start and end apart: 10, of which 9 were waited for; matrix products, arithmetic and copies ran while one was open for 5% of the time, Pallas kernels for 0%

profile of v1, /device:TPU:192, one launch (start us, length us, event | category | flops | bytes accessed | tf_op | source)
XLA Modules:
  0.0 359.7 jit_solution(6491564052675328995)
XLA Ops:
  0.0 1.0 fusion.59
  4.7 1.1 broadcast_in_dim.12
  5.8 14.0 %all-to-all-start = ((f32[64,5,512]{2,1,0:T(8,128)}), f32[64,5,512]{2,1,0:T(8,128)S(1)}, u32[]{:S(2)}, u32[]{:S(2)}) async-start(f32[64,5,512]{2,1,0:T(8,128)} %broadcast_in_dim.12), calls=%async_computation | async-start | bytes 2097152 | tf_op jit(solution)/shard_map/all_to_all | solution.py:26
  19.9 1.5 fusion.16
  22.1 27.0 %all-to-all-done = f32[64,5,512]{2,1,0:T(8,128)S(1)} async-done(((f32[64,5,512]{2,1,0:T(8,128)}), f32[64,5,512]{2,1,0:T(8,128)S(1)}, u32[]{:S(2)}, u32[]{:S(2)}) %all-to-all-start) | async-done | bytes 655392 | tf_op jit(solution)/shard_map/all_to_all | solution.py:26
  49.8 4.3 %all-to-all-start.1 = ((f32[4,5,512]{2,1,0:T(8,128)}), f32[4,5,512]{2,1,0:T(8,128)S(1)}, u32[]{:S(2)}, u32[]{:S(2)}) async-start(f32[4,5,512]{2,1,0:T(8,128)} %broadcast_in_dim.13), calls=%async_computation.1 | async-start | bytes 131072 | tf_op jit(solution)/shard_map/all_to_all | solution.py:26
  54.1 5.6 %all-to-all-done.1 = f32[4,5,512]{2,1,0:T(8,128)S(1)} async-done(((f32[4,5,512]{2,1,0:T(8,128)}), f32[4,5,512]{2,1,0:T(8,128)S(1)}, u32[]{:S(2)}, u32[]{:S(2)}) %all-to-all-start.1) | async-done | bytes 40992 | tf_op jit(solution)/shard_map/all_to_all | solution.py:26
  60.4 1.6 convolution_convert_fusion.1
  62.0 1.3 multiply_reduce_fusion.2
  64.3 3.4 collective-permute-start
  67.7 2.7 collective-permute-done
  70.5 1.9 collective-permute-start.1
  72.4 7.3 %collective-permute-done.1 = bf16[512,128]{0,1:T(8,128)(2,1)S(1)} collective-permute-done((bf16[512,128]{0,1:T(8,128)(2,1)S(1)}, bf16[512,128]{0,1:T(8,128)(2,1)S(1)}, u32[]{:S(2)}, u32[]{:S(2)}) %collective-permute-start.1) | collective-permute-done | bytes 131104 | tf_op jit(solution)/shard_map/ppermute | solution.py:16
  79.8 3.7 %collective-permute-start.2 = (bf16[1024,128]{0,1:T(8,128)(2,1)S(1)}, bf16[1024,128]{0,1:T(8,128)(2,1)S(1)}, u32[]{:S(2)}, u32[]{:S(2)}) collective-permute-start(bf16[1024,128]{0,1:T(8,128)(2,1)S(1)} %maximum_select_fusion.4), channel_id=1, source_target_pairs={{0,32},{8,40},{16,48},{24,56},{32,0},{40,8},{48,16},{56,24},{64,96... | collective-permute-start | bytes 786440 | tf_op jit(solution)/shard_map/ppermute | solution.py:16
  83.5 8.9 %collective-permute-done.2 = bf16[1024,128]{0,1:T(8,128)(2,1)S(1)} collective-permute-done((bf16[1024,128]{0,1:T(8,128)(2,1)S(1)}, bf16[1024,128]{0,1:T(8,128)(2,1)S(1)}, u32[]{:S(2)}, u32[]{:S(2)}) %collective-permute-start.2) | collective-permute-done | bytes 262176 | tf_op jit(solution)/shard_map/ppermute | solution.py:16
  92.6 5.6 %collective-permute-start.3 = (bf16[2048,128]{0,1:T(8,128)(2,1)S(1)}, bf16[2048,128]{0,1:T(8,128)(2,1)S(1)}, u32[]{:S(2)}, u32[]{:S(2)}) collective-permute-start(bf16[2048,128]{0,1:T(8,128)(2,1)S(1)} %maximum_select_fusion.3), channel_id=1, source_target_pairs={{0,64},{8,72},{16,80},{24,88},{32,96},{40,104},{48,112},{56,120},{... | collective-permute-start | bytes 1572872 | tf_op jit(solution)/shard_map/ppermute | solution.py:16
  99.6 9.1 %collective-permute-done.3 = bf16[2048,128]{0,1:T(8,128)(2,1)S(1)} collective-permute-done((bf16[2048,128]{0,1:T(8,128)(2,1)S(1)}, bf16[2048,128]{0,1:T(8,128)(2,1)S(1)}, u32[]{:S(2)}, u32[]{:S(2)}) %collective-permute-start.3) | collective-permute-done | bytes 524320 | tf_op jit(solution)/shard_map/ppermute | solution.py:16
  108.9 1.9 collective-permute-start.4
  111.8 1.3 copy.41
  113.0 2.3 copy.33
  115.3 1.0 multiply_reduce_fusion.3
  117.1 1.2 convolution_convert_fusion.2
  119.2 11.2 %all-to-all-start.2 = ((bf16[64,16,128]{2,1,0:T(8,128)(2,1)}), bf16[64,16,128]{2,1,0:T(8,128)(2,1)S(1)}, u32[]{:S(2)}, u32[]{:S(2)}) async-start(bf16[64,16,128]{2,1,0:T(8,128)(2,1)} %broadcast_in_dim.14), calls=%async_computation.2 | async-start | bytes 524288 | tf_op jit(solution)/shard_map/all_to_all | solution.py:26
  130.4 24.1 %collective-permute-done.4 = bf16[4096,128]{0,1:T(8,128)(2,1)} collective-permute-done((bf16[4096,128]{0,1:T(8,128)(2,1)S(1)}, bf16[4096,128]{0,1:T(8,128)(2,1)}, u32[]{:S(2)}, u32[]{:S(2)}) %collective-permute-start.4) | collective-permute-done | bytes 1048608 | tf_op jit(solution)/shard_map/ppermute | solution.py:16
  154.5 3.3 maximum_select_fusion.1
  157.9 3.9 %collective-permute-start.5 = (bf16[8192,128]{0,1:T(8,128)(2,1)}, bf16[8192,128]{0,1:T(8,128)(2,1)}, u32[]{:S(2)}, u32[]{:S(2)}) collective-permute-start(bf16[8192,128]{0,1:T(8,128)(2,1)} %maximum_select_fusion.1), channel_id=1, source_target_pairs={{0,256},{8,264},{16,272},{24,280},{32,288},{40,296},{48,304},{56,3... | collective-permute-start | bytes 6291464 | tf_op jit(solution)/shard_map/ppermute | solution.py:16
  164.5 1.0 fusion.25
  165.6 88.5 %collective-permute-done.5 = bf16[8192,128]{0,1:T(8,128)(2,1)} collective-permute-done((bf16[8192,128]{0,1:T(8,128)(2,1)}, bf16[8192,128]{0,1:T(8,128)(2,1)}, u32[]{:S(2)}, u32[]{:S(2)}) %collective-permute-start.5) | collective-permute-done | bytes 2097184 | tf_op jit(solution)/shard_map/ppermute | solution.py:16
  254.1 6.0 %maximum_select_fusion = bf16[16384,128]{0,1:T(8,128)(2,1)} fusion(bf16[8192,128]{0,1:T(8,128)(2,1)} %collective-permute-done.5, bf16[8192,128]{0,1:T(8,128)(2,1)} %maximum_select_fusion.1, pred[]{:T(512)S(6)} %eq.20), kind=kLoop, calls=%fused_computation.13 | loop fusion | flops 18874368 | bytes 8388609 | tf_op jit(solution)/shard_map/jit(_where)/select_n | solution.py:19
  260.1 6.4 %copy.38 = bf16[16384,128]{1,0:T(8,128)(2,1)} copy(bf16[16384,128]{0,1:T(8,128)(2,1)} %maximum_select_fusion) | data formatting | bytes 8388608 | tf_op jit(solution)/shard_map/while | solution.py:197
  266.4 54.7 %while.14 = (s32[]{:T(128)}, f32[1024]{0:T(1024)S(1)}, f32[1024]{0:T(1024)S(1)}, f32[1024,64]{0,1:T(8,128)S(1)}, bf16[16,1024,128]{2,1,0:T(8,128)(2,1)}, /*index=5*/bf16[1024,64]{1,0:T(8,128)(2,1)S(1)}, s32[]{:T(128)}) while((s32[]{:T(128)}, f32[1024]{0:T(1024)S(1)}, f32[1024]{0:T(1024)S(1)}, f32[1024,64]{0,1:T(8,128)S(1)}, ...), condition=%wide.region_11.12_spmd, body=%wide.region_8.11_spmd.sunk | while | flops 276957184 | bytes 14352473 | solution.py:197
  269.8 1.0 dynamic-slice_bitcast_fusion.2
  276.7 1.0 dynamic-slice_bitcast_fusion.2
  280.1 1.0 dynamic-slice_bitcast_fusion.2
  283.5 1.0 dynamic-slice_bitcast_fusion.2
  286.9 1.0 dynamic-slice_bitcast_fusion.2
  290.4 1.0 dynamic-slice_bitcast_fusion.2
  293.8 1.0 dynamic-slice_bitcast_fusion.2
  297.2 1.0 dynamic-slice_bitcast_fusion.2
  300.6 1.0 dynamic-slice_bitcast_fusion.2
  304.0 1.0 dynamic-slice_bitcast_fusion.2
  307.5 1.0 dynamic-slice_bitcast_fusion.2
  310.9 1.0 dynamic-slice_bitcast_fusion.2
  314.3 1.0 dynamic-slice_bitcast_fusion.2
  321.3 1.4 convolution_convert_fusion
  322.7 3.5 all-to-all-start.3
  326.2 15.2 %all-to-all-done.3 = bf16[4,64,2048]{2,1,0:T(8,128)(2,1)S(1)} async-done(((bf16[4,64,2048]{2,1,0:T(8,128)(2,1)}), bf16[4,64,2048]{2,1,0:T(8,128)(2,1)S(1)}, u32[]{:S(2)}, u32[]{:S(2)}) %all-to-all-start.3) | async-done | bytes 1048608 | tf_op jit(solution)/shard_map/all_to_all | solution.py:53
  341.8 16.8 %all_to_all.25 = bf16[4,64,2048]{2,1,0:T(8,128)(2,1)S(1)} all-to-all(bf16[4,64,2048]{2,1,0:T(8,128)(2,1)S(1)} %broadcast_in_dim.17), channel_id=1, replica_groups=mesh['sp'=64,'tp'=4,'dp'=2] {'tp'}, dimensions={0} | all-to-all | bytes 2097152 | tf_op jit(solution)/shard_map/all_to_all | solution.py:26
  (182 shorter events, 56.2 us)
Async XLA Ops:
  0.0 321.3 %copy-start = (bf16[256,2048]{1,0:T(8,128)(2,1)S(1)}, bf16[256,2048]{1,0:T(8,128)(2,1)}, u32[]{:S(2)}) copy-start(bf16[256,2048]{1,0:T(8,128)(2,1)} %param.28) | copy-start | bytes 3145732
  0.0 60.4 %copy-start.1 = (bf16[1,256,2048]{2,1,0:T(8,128)(2,1)S(1)}, bf16[1,256,2048]{2,1,0:T(8,128)(2,1)}, u32[]{:S(2)}) copy-start(bf16[1,256,2048]{2,1,0:T(8,128)(2,1)} %param.17) | copy-start | bytes 3145732
  0.0 60.4 %copy-start.9 = (f32[2048]{0:T(1024)S(1)}, f32[2048]{0:T(1024)}, u32[]{:S(2)}) copy-start(f32[2048]{0:T(1024)} %param.24) | copy-start | bytes 24580
  4.7 57.3 %copy-start.4 = (bf16[2048,64]{0,1:T(8,128)(2,1)S(1)}, bf16[2048,64]{0,1:T(8,128)(2,1)}, u32[]{:S(2)}) copy-start(bf16[2048,64]{0,1:T(8,128)(2,1)} %param.26) | copy-start | bytes 786436
  5.8 43.2 %all-to-all-start = ((f32[64,5,512]{2,1,0:T(8,128)}), f32[64,5,512]{2,1,0:T(8,128)S(1)}, u32[]{:S(2)}, u32[]{:S(2)}) async-start(f32[64,5,512]{2,1,0:T(8,128)} %broadcast_in_dim.12), calls=%async_computation | async-start | bytes 2097152 | tf_op jit(solution)/shard_map/all_to_all | solution.py:26
  49.2 14.9 %copy-start.5 = (f32[256,1,16]{0,2,1:T(8,128)S(1)}, f32[256,1,16]{0,2,1:T(8,128)}, u32[]{:S(2)}) copy-start(f32[256,1,16]{0,2,1:T(8,128)} %get-tuple-element.97) | copy-start | bytes 49156
  49.2 14.9 %copy-start.6 = (f32[256,1,16]{0,2,1:T(8,128)S(1)}, f32[256,1,16]{0,2,1:T(8,128)}, u32[]{:S(2)}) copy-start(f32[256,1,16]{0,2,1:T(8,128)} %get-tuple-element.102) | copy-start | bytes 49156
  49.8 9.9 %all-to-all-start.1 = ((f32[4,5,512]{2,1,0:T(8,128)}), f32[4,5,512]{2,1,0:T(8,128)S(1)}, u32[]{:S(2)}, u32[]{:S(2)}) async-start(f32[4,5,512]{2,1,0:T(8,128)} %broadcast_in_dim.13), calls=%async_computation.1 | async-start | bytes 131072 | tf_op jit(solution)/shard_map/all_to_all | solution.py:26
  54.1 9.2 %copy-start.15 = (f32[256]{0:T(256)}, f32[256]{0:T(256)S(1)}, u32[]{:S(2)}) copy-start(f32[256]{0:T(256)S(1)} %add_rsqrt_fusion.2) | copy-start | bytes 3076
  60.4 3.9 %copy-start.11 = (f32[1,4,512]{2,0,1:T(1,128)}, f32[1,4,512]{2,0,1:T(1,128)S(1)}, u32[]{:S(2)}) copy-start(f32[1,4,512]{2,0,1:T(1,128)S(1)} %get-tuple-element.93) | copy-start | bytes 24580
  60.4 3.9 %copy-start.13 = (f32[1,4,512]{2,0,1:T(1,128)}, f32[1,4,512]{2,0,1:T(1,128)S(1)}, u32[]{:S(2)}) copy-start(f32[1,4,512]{2,0,1:T(1,128)S(1)} %get-tuple-element.94) | copy-start | bytes 24580
  60.4 37.8 %copy-start.3 = (bf16[1,16,2048]{2,1,0:T(8,128)(2,1)S(1)}, bf16[1,16,2048]{2,1,0:T(8,128)(2,1)}, u32[]{:S(2)}) copy-start(bf16[1,16,2048]{2,1,0:T(8,128)(2,1)} %param.19) | copy-start | bytes 196612
  60.4 38.5 %copy-start.18 = (f32[4]{0:T(128)S(1)}, f32[4]{0:T(128)}, u32[]{:S(2)}) copy-start(f32[4]{0:T(128)} %param.31) | copy-start | bytes 52
  64.3 6.2 %collective-permute-start = (bf16[256,128]{0,1:T(8,128)(2,1)S(1)}, bf16[256,128]{0,1:T(8,128)(2,1)S(1)}, u32[]{:S(2)}, u32[]{:S(2)}) collective-permute-start(bf16[256,128]{0,1:T(8,128)(2,1)S(1)} %pad_maximum_fusion), channel_id=1, source_target_pairs={{0,8},{8,0},{16,24},{24,16},{32,40},{40,32},{48,56},{56,48},{64,72... | collective-permute-start | bytes 196616 | tf_op jit(solution)/shard_map/ppermute | solution.py:16
  70.5 9.3 %collective-permute-start.1 = (bf16[512,128]{0,1:T(8,128)(2,1)S(1)}, bf16[512,128]{0,1:T(8,128)(2,1)S(1)}, u32[]{:S(2)}, u32[]{:S(2)}) collective-permute-start(bf16[512,128]{0,1:T(8,128)(2,1)S(1)} %maximum_select_fusion.5), channel_id=1, source_target_pairs={{0,16},{8,24},{16,0},{24,8},{32,48},{40,56},{48,32},{56,40},{64,80... | collective-permute-start | bytes 393224 | tf_op jit(solution)/shard_map/ppermute | solution.py:16
  79.8 12.6 %collective-permute-start.2 = (bf16[1024,128]{0,1:T(8,128)(2,1)S(1)}, bf16[1024,128]{0,1:T(8,128)(2,1)S(1)}, u32[]{:S(2)}, u32[]{:S(2)}) collective-permute-start(bf16[1024,128]{0,1:T(8,128)(2,1)S(1)} %maximum_select_fusion.4), channel_id=1, source_target_pairs={{0,32},{8,40},{16,48},{24,56},{32,0},{40,8},{48,16},{56,24},{64,96... | collective-permute-start | bytes 786440 | tf_op jit(solution)/shard_map/ppermute | solution.py:16
  92.6 16.1 %collective-permute-start.3 = (bf16[2048,128]{0,1:T(8,128)(2,1)S(1)}, bf16[2048,128]{0,1:T(8,128)(2,1)S(1)}, u32[]{:S(2)}, u32[]{:S(2)}) collective-permute-start(bf16[2048,128]{0,1:T(8,128)(2,1)S(1)} %maximum_select_fusion.3), channel_id=1, source_target_pairs={{0,64},{8,72},{16,80},{24,88},{32,96},{40,104},{48,112},{56,120},{... | collective-permute-start | bytes 1572872 | tf_op jit(solution)/shard_map/ppermute | solution.py:16
  108.9 45.6 %collective-permute-start.4 = (bf16[4096,128]{0,1:T(8,128)(2,1)S(1)}, bf16[4096,128]{0,1:T(8,128)(2,1)}, u32[]{:S(2)}, u32[]{:S(2)}) collective-permute-start(bf16[4096,128]{0,1:T(8,128)(2,1)S(1)} %maximum_select_fusion.2), channel_id=1, source_target_pairs={{0,128},{8,136},{16,144},{24,152},{32,160},{40,168},{48,176},{56,1... | collective-permute-start | bytes 3145736 | tf_op jit(solution)/shard_map/ppermute | solution.py:16
  116.3 45.5 %copy-start.10 = (f32[2048]{0:T(1024)S(1)}, f32[2048]{0:T(1024)}, u32[]{:S(2)}) copy-start(f32[2048]{0:T(1024)} %param.24) | copy-start | bytes 24580
  116.4 45.5 %copy-start.12 = (f32[1,4,512]{2,0,1:T(1,128)S(1)}, f32[1,4,512]{2,0,1:T(1,128)}, u32[]{:S(2)}) copy-start(f32[1,4,512]{2,0,1:T(1,128)} %copy-done.11) | copy-start | bytes 24580
  116.4 45.5 %copy-start.14 = (f32[1,4,512]{2,0,1:T(1,128)S(1)}, f32[1,4,512]{2,0,1:T(1,128)}, u32[]{:S(2)}) copy-start(f32[1,4,512]{2,0,1:T(1,128)} %copy-done.13) | copy-start | bytes 24580
  116.4 45.5 %copy-start.16 = (f32[256]{0:T(256)S(1)}, f32[256]{0:T(256)}, u32[]{:S(2)}) copy-start(f32[256]{0:T(256)} %copy-done.15) | copy-start | bytes 3076
  119.2 43.8 %all-to-all-start.2 = ((bf16[64,16,128]{2,1,0:T(8,128)(2,1)}), bf16[64,16,128]{2,1,0:T(8,128)(2,1)S(1)}, u32[]{:S(2)}, u32[]{:S(2)}) async-start(bf16[64,16,128]{2,1,0:T(8,128)(2,1)} %broadcast_in_dim.14), calls=%async_computation.2 | async-start | bytes 524288 | tf_op jit(solution)/shard_map/all_to_all | solution.py:26
  130.4 31.5 %copy-start.2 = (bf16[2048,256]{0,1:T(8,128)(2,1)S(1)}, bf16[2048,256]{0,1:T(8,128)(2,1)}, u32[]{:S(2)}) copy-start(bf16[2048,256]{0,1:T(8,128)(2,1)} %copy.33) | copy-start | bytes 3145732
  130.4 32.2 %copy-start.17 = (f32[64]{0:T(128)S(1)}, f32[64]{0:T(128)}, u32[]{:S(2)}) copy-start(f32[64]{0:T(128)} %param.29) | copy-start | bytes 772
  157.9 5.1 %copy-start.7 = (f32[1,2,4,128]{3,1,2,0:T(2,128)S(1)}, f32[1,2,4,128]{3,1,2,0:T(2,128)}, u32[]{:S(2)}) copy-start(f32[1,2,4,128]{3,1,2,0:T(2,128)} %copy.41) | copy-start | bytes 12292
  157.9 96.2 %collective-permute-start.5 = (bf16[8192,128]{0,1:T(8,128)(2,1)}, bf16[8192,128]{0,1:T(8,128)(2,1)}, u32[]{:S(2)}, u32[]{:S(2)}) collective-permute-start(bf16[8192,128]{0,1:T(8,128)(2,1)} %maximum_select_fusion.1), channel_id=1, source_target_pairs={{0,256},{8,264},{16,272},{24,280},{32,288},{40,296},{48,304},{56,3... | collective-permute-start | bytes 6291464 | tf_op jit(solution)/shard_map/ppermute | solution.py:16
  321.1 20.5 %copy-start.8 = (f32[1,4,512]{2,0,1:T(1,128)S(1)}, f32[1,4,512]{2,0,1:T(1,128)}, u32[]{:S(2)}) copy-start(f32[1,4,512]{2,0,1:T(1,128)} %get-tuple-element.90) | copy-start | bytes 24580
  322.7 18.8 %all-to-all-start.3 = ((bf16[4,64,2048]{2,1,0:T(8,128)(2,1)}), bf16[4,64,2048]{2,1,0:T(8,128)(2,1)S(1)}, u32[]{:S(2)}, u32[]{:S(2)}) async-start(bf16[4,64,2048]{2,1,0:T(8,128)(2,1)} %bitcast.36), calls=%async_computation.3 | async-start | bytes 2097152 | tf_op jit(solution)/shard_map/all_to_all | solution.py:53
